TPU v7x, 32 devices: a whole 2x2x4 slice. The times are simulated.
32 devices in a mesh: grp: 2 (over x), ep: 16 (over z, y, core).
Axes of the slice: x: 2, y: 2, z: 4, core: 2. Of those that a mesh axis runs over, the one named last changes fastest.
Arguments:
- tokens: bfloat16 [1024, 2048], P(('grp', 'ep')), parts along dimension 0, may hold values from -6 to 6
- routing: int32 [1024, 4], P(('grp', 'ep')), parts along dimension 0, may hold values from 0 to 15, as said below
- gate_weights: float32 [1024, 4], P(('grp', 'ep')), parts along dimension 0, may hold values from 0.05 to 1
- pre_gain: float32 [2048], replicated, may hold values from 0.1 to 1.9
- w_gate: bfloat16 [16, 2048, 512], P('ep'), may hold values from -0.125 to 0.125
- w_up: bfloat16 [16, 2048, 512], P('ep'), may hold values from -0.125 to 0.125
- w_down: bfloat16 [16, 512, 2048], P('ep'), may hold values from -0.25 to 0.25
- post_gain: float32 [2048], replicated, may hold values from 0.1 to 1.9
Outputs:
- mixed_out: bfloat16 [1024, 2048], P(('grp', 'ep')), parts along dimension 0
There are 2 independent parts, one for each index of `grp`. A program takes and returns all parts, laid end to end along the dimension named above; an argument that names none is the same for every part. Nothing has to cross between parts.
Inputs may be any that keep to these rules, and one draw needn't show every extreme that they name: `routing`: each row names 4 different experts of one group (experts g * 8 to g * 8 + 7). The rows of one device name any one expert at most 16 times, and some expert exactly 16 times.
All inputs are finite; a program needn't handle non-finite values.
Results may differ from a plain program's by a relative error of at most 0.0085.
Values may be sent and summed in bfloat16 or wider, within the bound.
A program may use at most 64 MiB of HBM per device.

v0:
```python
import jax
import jax.numpy as jnp
from jax import lax
from jax.sharding import PartitionSpec as P

epsilon = 1e-06


def normalize(values, gain):
    floats = values.astype(jnp.float32)
    return floats * lax.rsqrt(jnp.mean(floats * floats, axis=-1, keepdims=True) + epsilon) * gain


def apply_expert(rows, w_gate, w_up, w_down):
    gate = jnp.dot(rows, w_gate[0], preferred_element_type=jnp.float32)
    upward = jnp.dot(rows, w_up[0], preferred_element_type=jnp.float32)
    hidden = (jax.nn.silu(gate) * upward).astype(jnp.bfloat16)
    return jnp.dot(hidden, w_down[0], preferred_element_type=jnp.float32).astype(jnp.bfloat16)


def body(tokens, routing, gate_weights, pre_gain, w_gate, w_up, w_down, post_gain):
    normed = normalize(tokens, pre_gain).astype(jnp.bfloat16)
    tok_rows, choices_count = routing.shape
    width = tokens.shape[1]
    devices = lax.axis_size("ep")
    capacity = tok_rows * choices_count * 2 // devices
    flat_expert = routing.reshape(-1)
    one_hot = (flat_expert[:, None] == jnp.arange(devices, dtype=jnp.int32)[None, :]).astype(
        jnp.int32
    )
    ranking = jnp.sum((jnp.cumsum(one_hot, axis=0) - one_hot) * one_hot, axis=1)
    destination = flat_expert * capacity + ranking
    flat_token = jnp.repeat(jnp.arange(tok_rows, dtype=jnp.int32), choices_count)
    outbox = (
        jnp.zeros((devices * capacity, width), jnp.bfloat16).at[destination].set(normed[flat_token])
    )
    outbox = outbox.reshape(devices, capacity, width)
    received = lax.all_to_all(outbox, "ep", split_axis=0, concat_axis=0, tiled=True)
    served = apply_expert(received.reshape(-1, width), w_gate, w_up, w_down).reshape(received.shape)
    returned = lax.all_to_all(served, "ep", split_axis=0, concat_axis=0, tiled=True)
    gathered_rows = returned.reshape(devices * capacity, width)[destination].reshape(
        tok_rows, choices_count, width
    )
    mixture = jnp.einsum("tk,tkd->td", gate_weights, gathered_rows.astype(jnp.float32))
    return normalize(mixture, post_gain).astype(jnp.bfloat16)


def solution(mesh):
    in_specs = (
        P(("grp", "ep"), None),
        P(("grp", "ep"), None),
        P(("grp", "ep"), None),
        P(),
        P("ep", None, None),
        P("ep", None, None),
        P("ep", None, None),
        P(),
    )
    out_specs = P(("grp", "ep"), None)
    return jax.shard_map(body, mesh=mesh, in_specs=in_specs, out_specs=out_specs, check_vma=False)
```

profile of v0, /device:TPU:11, one launch (start us, length us, event | category | flops | bytes accessed | tf_op | source)
XLA Modules:
  0.0 79.6 jit_solution(15481507811709905725)
XLA Ops:
  0.0 0.0 copy-start
  0.0 0.9 %copy.12 = s32[32,4]{1,0:T(8,128)S(1)} copy(s32[32,4]{0,1:T(4,128)} %param.9) | data formatting | bytes 1024 | tf_op args[1]
  0.9 0.7 broadcast_multiply_fusion
  1.6 0.1 eq.15
  1.7 0.1 fusion.28
  1.8 0.2 reduce_window_sum.11
  2.0 0.2 select_reduce_fusion
  2.1 0.1 copy.11
  2.2 0.1 mul.66
  2.3 1.0 %fusion.21 = f32[32]{0:T(128)S(1)} fusion(bf16[32,2048]{1,0:T(8,128)(2,1)} %param.8), kind=kLoop, calls=%fused_computation.21 | loop fusion | flops 196576 | bytes 131200 | tf_op jit(solution)/shard_map/reduce_sum | solution.py:11
  3.4 0.1 reshape.94
  3.6 1.0 %fusion.23 = bf16[32,2048]{1,0:T(8,128)(2,1)S(1)} fusion(bf16[32,2048]{1,0:T(8,128)(2,1)} %param.8, f32[2048]{0:T(1024)} %param.11, f32[32]{0:T(128)S(1)} %add_rsqrt_fusion.1), kind=kLoop, calls=%fused_computation.23 | loop fusion | flops 262144 | bytes 270464 | tf_op jit(solution)/shard_map/convert_element_type | solution.py:22
  4.6 3.4 %scatter_custom_fusion = bf16[256,2048]{1,0:T(8,128)(2,1)S(1)} fusion(s32[128]{0:T(128)S(1)} %fusion.29, bf16[32,2048]{1,0:T(8,128)(2,1)S(1)} %fusion.23, s32[1024]{0:T(1024)S(1)} %pad_clamp_fusion.1, bf16[]{:T(256)} %constant.9.clone.1), kind=kCustom, calls=%fused_computation.11 | custom fusion | bytes 1048578 | tf_op jit(solution)/shard_map/scatter | solution.py:35
  7.9 0.0 copy-start.4
  7.9 31.9 %all_to_all.10 = bf16[16,16,2048]{2,1,0:T(8,128)(2,1)S(1)} all-to-all(bf16[16,16,2048]{2,1,0:T(8,128)(2,1)S(1)} %bitcast.42), channel_id=1, replica_groups=mesh['grp'=2,'ep'=16] {'ep'}, dimensions={0} | all-to-all | bytes 2097152 | tf_op jit(solution)/shard_map/all_to_all | solution.py:38
  39.8 0.0 copy-start.1
  39.8 1.0 %copy-done.1 = bf16[16,16,2048]{2,1,0:T(8,128)(2,1)} copy-done((bf16[16,16,2048]{2,1,0:T(8,128)(2,1)}, bf16[16,16,2048]{2,1,0:T(8,128)(2,1)S(1)}, u32[]{:S(2)}) %copy-start.1) | copy-done | bytes 1048600
  40.8 0.0 copy-done.4
  40.8 0.7 fusion.3
  41.5 0.0 copy-done
  41.5 4.3 %convolution_convert_fusion = bf16[256,2048]{1,0:T(8,128)(2,1)} fusion(bf16[1,512,2048]{2,1,0:T(8,128)(2,1)S(1)} %copy-done, bf16[256,2048]{1,0:T(8,128)(2,1)} %bitcast.45, bf16[1,2048,512]{2,1,0:T(8,128)(2,1)} %param.13, f32[256,512]{1,0:T(8,128)S(1)} %fusion.3), kind=kOutput, calls=%fused_computation.3 | convolution fusion | flops 1075052544 | bytes 6815744 | tf_op jit(solution)/shard_map/dot_general | solution.py:18
  45.8 0.0 copy-start.3
  45.8 4.5 %all-to-all-start.1 = ((bf16[16,16,2048]{2,1,0:T(8,128)(2,1)}), bf16[16,16,2048]{2,1,0:T(8,128)(2,1)S(1)}, u32[]{:S(2)}, u32[]{:S(2)}) async-start(bf16[16,16,2048]{2,1,0:T(8,128)(2,1)} %bitcast.43), calls=%async_computation.1 | async-start | bytes 2097152 | tf_op jit(solution)/shard_map/all_to_all | solution.py:40
  50.3 0.0 copy-done.3
  50.3 0.1 copy.13
  50.4 24.8 %all-to-all-done.1 = bf16[16,16,2048]{2,1,0:T(8,128)(2,1)S(1)} async-done(((bf16[16,16,2048]{2,1,0:T(8,128)(2,1)}), bf16[16,16,2048]{2,1,0:T(8,128)(2,1)S(1)}, u32[]{:S(2)}, u32[]{:S(2)}) %all-to-all-start.1) | async-done | bytes 1048608 | tf_op jit(solution)/shard_map/all_to_all | solution.py:40
  75.3 1.7 %gather_fusion = bf16[128,2048]{1,0:T(8,128)(2,1)} fusion(bf16[256,2048]{1,0:T(8,128)(2,1)S(1)} %bitcast.41, s32[1024]{0:T(1024)S(1)} %pad_clamp_fusion), kind=kCustom, calls=%fused_computation.1 | custom fusion | bytes 1049088 | tf_op jit(solution)/shard_map/gather | solution.py:41
  77.0 1.2 %reshape.99 = bf16[32,4,2048]{2,1,0:T(4,128)(2,1)S(1)} reshape(bf16[128,2048]{1,0:T(8,128)(2,1)} %gather_fusion) | data formatting | bytes 1048576 | tf_op jit(solution)/shard_map/reshape | solution.py:41
  78.2 0.4 fusion.32
  78.7 0.2 fusion.24
  78.8 0.0 copy-done.2
  78.8 0.8 fusion.26
  (8 shorter events, 0.0 us)
Async XLA Ops:
  0.0 41.5 %copy-start = (bf16[1,512,2048]{2,1,0:T(8,128)(2,1)S(1)}, bf16[1,512,2048]{2,1,0:T(8,128)(2,1)}, u32[]{:S(2)}) copy-start(bf16[1,512,2048]{2,1,0:T(8,128)(2,1)} %param.14) | copy-start | bytes 6291460
  7.9 32.9 %copy-start.4 = (bf16[1,2048,512]{2,1,0:T(8,128)(2,1)S(1)}, bf16[1,2048,512]{2,1,0:T(8,128)(2,1)}, u32[]{:S(2)}) copy-start(bf16[1,2048,512]{2,1,0:T(8,128)(2,1)} %param.12) | copy-start | bytes 6291460
  39.8 1.0 %copy-start.1 = (bf16[16,16,2048]{2,1,0:T(8,128)(2,1)}, bf16[16,16,2048]{2,1,0:T(8,128)(2,1)S(1)}, u32[]{:S(2)}) copy-start(bf16[16,16,2048]{2,1,0:T(8,128)(2,1)S(1)} %all_to_all.10) | copy-start | bytes 3145732
  45.8 4.5 %copy-start.3 = (f32[32,4]{0,1:T(4,128)S(1)}, f32[32,4]{0,1:T(4,128)}, u32[]{:S(2)}) copy-start(f32[32,4]{0,1:T(4,128)} %param.10) | copy-start | bytes 1540
  45.8 29.4 %all-to-all-start.1 = ((bf16[16,16,2048]{2,1,0:T(8,128)(2,1)}), bf16[16,16,2048]{2,1,0:T(8,128)(2,1)S(1)}, u32[]{:S(2)}, u32[]{:S(2)}) async-start(bf16[16,16,2048]{2,1,0:T(8,128)(2,1)} %bitcast.43), calls=%async_computation.1 | async-start | bytes 2097152 | tf_op jit(solution)/shard_map/all_to_all | solution.py:40
  77.0 1.9 %copy-start.2 = (f32[2048]{0:T(1024)S(1)}, f32[2048]{0:T(1024)}, u32[]{:S(2)}) copy-start(f32[2048]{0:T(1024)} %param.15) | copy-start | bytes 24580
where the time goes:
time: 80 us; the launch traced here: 79.6 us
  blocking collectives  31.9 us (40%)
  waiting for transfers between devices  24.8 us (31%)
  local copies, waits for them, and re-layouts  8.75 us (11%)
  matrix products  5.44 us (7%)
  starting transfers between devices  4.49 us (6%)
  other arithmetic  4.14 us (5%)
    all_to_all x1, blocking collectives, body(): lax.all_to_all(outbox, 'ep', split_axis=0, concat_axis=0, tiled=True)  31.9 us
    all_to_all x1, waiting for transfers between devices, body(): lax.all_to_all(served, 'ep', split_axis=0, concat_axis=0, tiled=True)  24.8 us
    all_to_all x1, starting transfers between devices, body(): lax.all_to_all(served, 'ep', split_axis=0, concat_axis=0, tiled=True)  4.49 us
    dot_general x1, matrix products, apply_expert(): jnp.dot(hidden, w_down[0], preferred_element_type=jnp.float32)  4.32 us
    scatter x1, local copies, waits for them, and re-layouts, body(): jnp.zeros((devices * capacity, width), jnp.bfloat16).at[destination]  3.36 us
    unnamed x12, local copies, waits for them, and re-layouts  2.02 us
    gather x1, local copies, waits for them, and re-layouts, body(): returned.reshape(devices * capacity, width)[destination]  1.72 us
  transfers between devices with their start and end apart: 1, of which 1 were waited for; matrix products, arithmetic and copies ran while one was open for 0% of the time, Pallas kernels for 0%

commit v1 on v0

v1 whole, which is shorter than its diff:
```python
import functools

import jax
import jax.numpy as jnp
from jax import lax
from jax.experimental import pallas as pl
from jax.experimental.pallas import tpu as pltpu
from jax.sharding import PartitionSpec as P

epsilon = 1e-06
MESH = pl.DeviceIdType.MESH


def kernel(
    n, tok, rout, gates, pre, wg_hbm, wu_hbm, wd_hbm, post, out,
    gath, part, rcore, ysend, ryy, zsend, rzz, acc, wg, wu, wd,
    ag_send, ag_recv, rs_core_s, rs_core_r, rs_y_s, rs_y_r, rs_z_s, rs_z_r, wsem,
):
    f32, bf16 = jnp.float32, jnp.bfloat16
    rows, width = tok.shape
    zs = n // 4
    me = lax.axis_index("ep")
    z, y, c = me // 4, (me // 2) % 2, me % 2

    def zx(d):
        value, bit = 0, 1
        while bit < zs:
            value = value + ((z // bit + (d // bit) % 2) % 2) * bit
            bit *= 2
        return value

    def dev(zz, yy, cc):
        return (zz * 2 + yy) * 2 + cc

    core_peer = dev(z, y, 1 - c)
    y_peer = dev(z, 1 - y, c)
    z_peer = [None] + [dev(zx(d), y, c) for d in range(1, zs)]

    loads = [
        pltpu.make_async_copy(src.at[0], dst, wsem.at[i])
        for i, (src, dst) in enumerate(((wg_hbm, wg), (wu_hbm, wu), (wd_hbm, wd)))
    ]
    for load in loads:
        load.start()

    barrier = pltpu.get_barrier_semaphore()
    for peer in [core_peer, y_peer] + z_peer[1:]:
        pl.semaphore_signal(barrier, inc=1, device_id={"ep": peer}, device_id_type=MESH)

    values = tok[...].astype(f32)
    scale = lax.rsqrt(jnp.mean(values * values, axis=-1, keepdims=True) + epsilon)
    gath[me, :, :width] = (values * scale * pre[...]).astype(bf16)
    extra = gath.shape[2] - width
    lane = lax.broadcasted_iota(jnp.int32, (rows, extra), 1)
    expert_of = jnp.where(lane < n, lane, lane - n)
    dense = jnp.zeros((rows, extra), f32)
    for k in range(rout.shape[1]):
        dense = dense + jnp.where(expert_of == rout[:, k : k + 1], gates[:, k : k + 1], 0.0)
    high = dense.astype(bf16).astype(f32)
    gath[me, :, width:] = jnp.where(lane < n, high, dense - high).astype(bf16)

    pl.semaphore_wait(barrier, zs + 1)

    def remote(src, dst, ssem, rsem, peer):
        return pltpu.make_async_remote_copy(
            src_ref=src, dst_ref=dst, send_sem=ssem, recv_sem=rsem,
            device_id={"ep": peer}, device_id_type=MESH,
        )

    started = []

    def go(copy):
        copy.start()
        started.append(copy)

    def slot(d, oy, oc):
        return dev(zx(d), y + oy - 2 * y * oy, c + oc - 2 * c * oc)

    def gcopy(d, oy, oc, i, peer):
        ref = gath.at[slot(d, oy, oc)]
        return remote(ref, ref, ag_send.at[i], ag_recv.at[i], peer)

    def gname(d, oy, oc):
        return (d * 2 + oy) * 2 + oc

    def gwait(d, oy, oc):
        gcopy(d, oy, oc, gname(d, oy, oc), core_peer).wait_recv()

    def forward_own(d):
        gwait(d, 0, 0)
        go(gcopy(d, 0, 0, gname(d, 1, 0), y_peer))
        go(gcopy(d, 0, 0, gname(d, 0, 1), core_peer))

    def forward_other(d):
        gwait(d, 1, 0)
        go(gcopy(d, 1, 0, gname(d, 1, 1), core_peer))

    def ffn(d):
        gwait(d, 0, 1)
        gwait(d, 1, 1)
        base = zx(d) * 4
        x = gath[pl.ds(base, 4), :, :width].reshape(4 * rows, width)
        gate = jnp.dot(x, wg[...], preferred_element_type=f32)
        up = jnp.dot(x, wu[...], preferred_element_type=f32)
        hidden = (gate / (1.0 + jnp.exp(-gate)) * up).astype(bf16)
        ext = gath[pl.ds(base, 4), :, width:].reshape(4 * rows, extra).astype(f32)
        lanes = lax.broadcasted_iota(jnp.int32, ext.shape, 1)
        mine = (lanes == me) | (lanes == me + n)
        weight = jnp.sum(jnp.where(mine, ext, 0.0), axis=-1, keepdims=True)
        served = jnp.dot(hidden, wd[...], preferred_element_type=f32) * weight
        part[d] = served.astype(bf16).reshape(4, rows, width)

    def core_copy(d, yy, cc):
        i = d * 2 + yy
        return remote(
            part.at[d, yy * 2 + cc], rcore.at[d, yy], rs_core_s.at[i], rs_core_r.at[i], core_peer
        )

    def send_core(d):
        for yy in range(2):
            go(core_copy(d, yy, 1 - c))

    def y_copy(d):
        return remote(ysend.at[d], ryy.at[d], rs_y_s.at[d], rs_y_r.at[d], y_peer)

    def send_y(d):
        for yy in range(2):
            core_copy(d, yy, 1 - c).wait_recv()
        oy = 1 - y
        ysend[d] = (part[d, oy * 2 + c].astype(f32) + rcore[d, oy].astype(f32)).astype(bf16)
        go(y_copy(d))

    def z_copy(d):
        return remote(zsend.at[d], rzz.at[d], rs_z_s.at[d], rs_z_r.at[d], z_peer[d])

    def send_z(d):
        y_copy(d).wait_recv()
        total = part[d, y * 2 + c].astype(f32) + rcore[d, y].astype(f32) + ryy[d].astype(f32)
        if d == 0:
            acc[...] = total
        else:
            zsend[d] = total.astype(bf16)
            go(z_copy(d))

    own = gath.at[me]
    go(remote(own, own, ag_send.at[gname(0, 1, 0)], ag_recv.at[gname(0, 1, 0)], y_peer))
    go(remote(own, own, ag_send.at[gname(0, 0, 1)], ag_recv.at[gname(0, 0, 1)], core_peer))
    for d in range(1, zs):
        i = gname(d, 0, 0)
        go(remote(own, own, ag_send.at[i], ag_recv.at[i], z_peer[d]))

    if zs > 1:
        forward_own(1)
    forward_other(0)
    for load in loads:
        load.wait()
    for d in range(zs):
        ffn(d)
        send_core(d)
        if d + 2 < zs:
            forward_own(d + 2)
        if d + 1 < zs:
            forward_other(d + 1)
        send_y(d)
        if d > 0:
            send_z(d - 1)
    send_z(zs - 1)
    total = acc[...]
    for d in range(1, zs):
        z_copy(d).wait_recv()
        total = total + rzz[d].astype(f32)
    scale = lax.rsqrt(jnp.mean(total * total, axis=-1, keepdims=True) + epsilon)
    out[...] = (total * scale * post[...]).astype(out.dtype)
    for copy in started:
        copy.wait_send()


def body(tokens, routing, gate_weights, pre_gain, w_gate, w_up, w_down, post_gain):
    n = lax.axis_size("ep")
    rows, width = tokens.shape
    ff = w_gate.shape[2]
    zs = n // 4
    extra = -(-2 * n // 128) * 128
    bf16, dma = jnp.bfloat16, pltpu.SemaphoreType.DMA
    vmem = pl.BlockSpec(memory_space=pltpu.VMEM)
    hbm = pl.BlockSpec(memory_space=pl.ANY)
    return pl.pallas_call(
        functools.partial(kernel, n),
        out_shape=jax.ShapeDtypeStruct((rows, width), bf16),
        in_specs=[vmem, vmem, vmem, vmem, hbm, hbm, hbm, vmem],
        out_specs=vmem,
        scratch_shapes=[
            pltpu.VMEM((n, rows, width + extra), bf16),
            pltpu.VMEM((zs, 4, rows, width), bf16),
            pltpu.VMEM((zs, 2, rows, width), bf16),
            pltpu.VMEM((zs, rows, width), bf16),
            pltpu.VMEM((zs, rows, width), bf16),
            pltpu.VMEM((zs, rows, width), bf16),
            pltpu.VMEM((zs, rows, width), bf16),
            pltpu.VMEM((rows, width), jnp.float32),
            pltpu.VMEM((width, ff), bf16),
            pltpu.VMEM((width, ff), bf16),
            pltpu.VMEM((ff, width), bf16),
            dma((n,)), dma((n,)),
            dma((2 * zs,)), dma((2 * zs,)),
            dma((zs,)), dma((zs,)), dma((zs,)), dma((zs,)),
            dma((3,)),
        ],
        compiler_params=pltpu.CompilerParams(
            collective_id=0, has_side_effects=True, vmem_limit_bytes=60 * 1024 * 1024
        ),
    )(
        tokens, routing, gate_weights, pre_gain.reshape(1, width),
        w_gate, w_up, w_down, post_gain.reshape(1, width),
    )


def solution(mesh):
    rows = P(("grp", "ep"), None)
    expert = P("ep", None, None)
    in_specs = (rows, rows, rows, P(), expert, expert, expert, P())
    return jax.shard_map(body, mesh=mesh, in_specs=in_specs, out_specs=rows, check_vma=False)
```

time: 80 us -> 47.7 us (0.60)
  Pallas kernels: 0 us -> 43.2 us
  blocking collectives: 31.9 us -> 0 us
  waiting for transfers between devices: 24.8 us -> 0 us
  matrix products: 5.44 us -> 0 us
  starting transfers between devices: 4.49 us -> 0 us
  local copies, waits for them, and re-layouts: 8.75 us -> 4.29 us
  other arithmetic: 4.14 us -> 0 us
    pallas_call x0 -> x1, Pallas kernels: none -> 43.2 us  [body(): pl.pallas_call(functools.partial(kernel, n), out_shape=jax.ShapeDtypeStru...]
    all_to_all x1 -> x0, blocking collectives: 31.9 us -> none  [body(): lax.all_to_all(outbox, 'ep', split_axis=0, concat_axis=0, tiled=True)]
    all_to_all x1 -> x0, waiting for transfers between devices: 24.8 us -> none  [body(): lax.all_to_all(served, 'ep', split_axis=0, concat_axis=0, tiled=True)]
    dot_general x3 -> x0, matrix products: 5.44 us -> none  [the longest x1 4.32 us: apply_expert(): jnp.dot(hidden, w_down[0], preferred_element_type=jnp.float32)]
    all_to_all x1 -> x0, starting transfers between devices: 4.49 us -> none  [body(): lax.all_to_all(served, 'ep', split_axis=0, concat_axis=0, tiled=True)]
    scatter x1 -> x0, local copies, waits for them, and re-layouts: 3.36 us -> none  [body(): jnp.zeros((devices * capacity, width), jnp.bfloat16).at[destination]]
    unnamed x12 -> x3, local copies, waits for them, and re-layouts: 2.02 us -> 4.29 us
    convert_element_type x3 -> x0, other arithmetic: 1.86 us -> none  [the longest x1 1.01 us: body(): normed = normalize(tokens, pre_gain).astype(jnp.bfloat16)]
  transfers between devices with their start and end apart: 1 -> 0, of which waited for: 1 -> 0; matrix products, arithmetic and copies ran while one was open for 0% -> 0% of each run, Pallas kernels for 0% -> 0%
where the time goes in v1:
time: 47.7 us; the launch traced here: 47.5 us
  Pallas kernels  43.2 us (91%)
  local copies, waits for them, and re-layouts  4.29 us (9%)
    pallas_call x1, Pallas kernels, body(): pl.pallas_call(functools.partial(kernel, n), out_shape=jax.ShapeDtypeStru...  43.2 us
    unnamed x3, local copies, waits for them, and re-layouts  4.29 us

profile of v1, /device:TPU:11, one launch (start us, length us, event | category | flops | bytes accessed | tf_op | source)
XLA Modules:
  0.0 47.5 jit_solution(6229837757467502871)
XLA Ops:
  0.0 1.4 %copy.9.rout = s32[32,4]{1,0:T(8,128)} copy(s32[32,4]{0,1:T(4,128)} %param.9) | data formatting | bytes 1024 | tf_op args[1]
  1.4 1.4 %copy.10.gates = f32[32,4]{1,0:T(8,128)} copy(f32[32,4]{0,1:T(4,128)} %param.10) | data formatting | bytes 1024 | tf_op args[2]
  2.7 43.2 %shard_map.82 = bf16[32,2048]{1,0:T(8,128)(2,1)} custom-call(bf16[32,2048]{1,0:T(8,128)(2,1)} %tok.1, s32[32,4]{1,0:T(8,128)} %copy.9.rout, f32[32,4]{1,0:T(8,128)} %copy.10.gates, f32[1,2048]{1,0:T(1,128)} %bitcast.2, bf16[1,2048,512]{2,1,0:T(8,128)(2,1)} %wg_hbm.1, bf16[1,2048,512]{2,1,0:T(8,128)(2,1)} %wu_hbm.1, bf16[1,512,2048]{2,1,0:T(8,128)(2,1)} %wd_hbm.1, ...), custom_call_target="tpu_custom_call" | custom-call | tf_op jit(solution)/shard_map/pallas_call | solution.py:187
  45.9 1.6 %copy.12 = bf16[32,2048]{1,0:T(8,128)(2,1)} copy(bf16[32,2048]{1,0:T(8,128)(2,1)} %shard_map.82) | data formatting | bytes 262144

commit v2 on v1

v2 whole, which is shorter than its diff:
```python
import functools

import jax
import jax.numpy as jnp
from jax import lax
from jax.experimental import pallas as pl
from jax.experimental.pallas import tpu as pltpu
from jax.sharding import PartitionSpec as P

epsilon = 1e-06
MESH = pl.DeviceIdType.MESH


def kernel(
    n, parts, tok, rout, gates, pre, wg_hbm, wu_hbm, wd_hbm, post, out,
    gath, part, rcore, ysend, ryy, zsend, rzz, acc, wg, wu, wd,
    ag_send, ag_recv, rs_core_s, rs_core_r, rs_y_s, rs_y_r, rs_z_s, rs_z_r, wsem,
):
    f32, bf16 = jnp.float32, jnp.bfloat16
    rows, width = tok.shape
    zs = n // 4
    me = lax.axis_index("ep")
    z, y, c = me // 4, (me // 2) % 2, me % 2

    def zx(d):
        value, bit = 0, 1
        while bit < zs:
            value = value + ((z // bit + (d // bit) % 2) % 2) * bit
            bit *= 2
        return value

    def dev(zz, yy, cc):
        return (zz * 2 + yy) * 2 + cc

    core_peer = dev(z, y, 1 - c)
    y_peer = dev(z, 1 - y, c)
    z_peer = [None] + [dev(zx(d), y, c) for d in range(1, zs)]

    loads = [
        pltpu.make_async_copy(src.at[0], dst, wsem.at[i])
        for i, (src, dst) in enumerate(((wg_hbm, wg), (wu_hbm, wu), (wd_hbm, wd)))
    ]
    for load in loads:
        load.start()

    barrier = pltpu.get_barrier_semaphore()
    for peer in [core_peer, y_peer] + z_peer[1:]:
        pl.semaphore_signal(barrier, inc=1, device_id={"ep": peer}, device_id_type=MESH)

    values = tok[...].astype(f32)
    scale = lax.rsqrt(jnp.mean(values * values, axis=-1, keepdims=True) + epsilon)
    normed = (values * scale * pre[...]).astype(bf16)
    extra = gath.shape[3] - width
    sub = lax.broadcasted_iota(jnp.int32, (extra, rows), 0)
    expert_of = jnp.where(sub < n, sub, sub - n)
    dense = jnp.zeros((extra, rows), f32)
    for k in range(rout.shape[0]):
        dense = dense + jnp.where(expert_of == rout[k : k + 1, :], gates[k : k + 1, :], 0.0)
    high = dense.astype(bf16).astype(f32)
    mixing = jnp.where(sub < n, high, dense - high).T.astype(bf16)
    piece = rows // parts
    for h in range(parts):
        gath[h, me, :, :width] = normed[h * piece : (h + 1) * piece]
        gath[h, me, :, width:] = mixing[h * piece : (h + 1) * piece]

    pl.semaphore_wait(barrier, zs + 1)

    def remote(src, dst, ssem, rsem, peer):
        return pltpu.make_async_remote_copy(
            src_ref=src, dst_ref=dst, send_sem=ssem, recv_sem=rsem,
            device_id={"ep": peer}, device_id_type=MESH,
        )

    started = []

    def go(copy):
        copy.start()
        started.append(copy)

    def slot(d, h, oy, oc):
        return gath.at[h, dev(zx(d), y + oy - 2 * y * oy, c + oc - 2 * c * oc)]

    def gname(d, h, oy, oc):
        return ((d * parts + h) * 2 + oy) * 2 + oc

    def gcopy(d, h, oy, oc, i, peer):
        ref = slot(d, h, oy, oc)
        return remote(ref, ref, ag_send.at[i], ag_recv.at[i], peer)

    def gwait(d, h, oy, oc):
        gcopy(d, h, oy, oc, gname(d, h, oy, oc), core_peer).wait_recv()

    def forward_own(d, h):
        if d > 0:
            gwait(d, h, 0, 0)
            go(gcopy(d, h, 0, 0, gname(d, h, 1, 0), y_peer))
            go(gcopy(d, h, 0, 0, gname(d, h, 0, 1), core_peer))

    def forward_other(d, h):
        gwait(d, h, 1, 0)
        go(gcopy(d, h, 1, 0, gname(d, h, 1, 1), core_peer))

    def at(d, h):
        return d * parts + h

    def core_copy(d, h, yy):
        i = at(d, h) * 2 + yy
        return remote(
            part.at[at(d, h), yy * 2 + 1 - c], rcore.at[at(d, h), yy],
            rs_core_s.at[i], rs_core_r.at[i], core_peer,
        )

    def ffn(d, h):
        gwait(d, h, 0, 1)
        gwait(d, h, 1, 1)
        base = zx(d) * 4
        x = gath[h, pl.ds(base, 4), :, :width].reshape(4 * piece, width)
        gate = jnp.dot(x, wg[...], preferred_element_type=f32)
        up = jnp.dot(x, wu[...], preferred_element_type=f32)
        hidden = (gate / (1.0 + jnp.exp(-gate)) * up).astype(bf16)
        ext = gath[h, pl.ds(base, 4), :, width:].reshape(4 * piece, extra).astype(f32)
        lanes = lax.broadcasted_iota(jnp.int32, ext.shape, 1)
        mine = (lanes == me) | (lanes == me + n)
        weight = jnp.sum(jnp.where(mine, ext, 0.0), axis=-1, keepdims=True)
        served = jnp.dot(hidden, wd[...], preferred_element_type=f32) * weight
        part[at(d, h)] = served.astype(bf16).reshape(4, piece, width)
        for yy in range(2):
            go(core_copy(d, h, yy))

    def y_copy(d, h):
        i = at(d, h)
        return remote(ysend.at[i], ryy.at[i], rs_y_s.at[i], rs_y_r.at[i], y_peer)

    def send_y(d, h):
        for yy in range(2):
            core_copy(d, h, yy).wait_recv()
        i, oy = at(d, h), 1 - y
        ysend[i] = (part[i, oy * 2 + c].astype(f32) + rcore[i, oy].astype(f32)).astype(bf16)
        go(y_copy(d, h))

    def z_copy(d, h):
        i = at(d, h)
        return remote(zsend.at[i], rzz.at[i], rs_z_s.at[i], rs_z_r.at[i], z_peer[d])

    def send_z(d, h):
        y_copy(d, h).wait_recv()
        i = at(d, h)
        total = part[i, y * 2 + c].astype(f32) + rcore[i, y].astype(f32) + ryy[i].astype(f32)
        if d == 0:
            acc[h] = total
        else:
            zsend[i] = total.astype(bf16)
            go(z_copy(d, h))

    order = ([0, 1] + list(range(2, zs))[::-1])[:zs]
    steps = [(d, h) for d in order for h in range(parts)]

    for h in range(parts):
        own = gath.at[h, me]
        for d, oy, oc, peer in ((0, 1, 0, y_peer), (0, 0, 1, core_peer)):
            i = gname(d, h, oy, oc)
            go(remote(own, own, ag_send.at[i], ag_recv.at[i], peer))
    for d, h in steps:
        if d > 0:
            i = gname(d, h, 0, 0)
            own = gath.at[h, me]
            go(remote(own, own, ag_send.at[i], ag_recv.at[i], z_peer[d]))
    for load in loads:
        load.wait()

    events = []
    for i, step in enumerate(steps):
        for lag, event in ((0, forward_own), (4, forward_other), (5.5, ffn), (8, send_y), (12.5, send_z)):
            events.append((4 * i / parts + lag, len(events), event, step))
    for _, _, event, step in sorted(events, key=lambda e: e[:2]):
        event(*step)

    for h in range(parts):
        total = acc[h]
        for d in order[1:]:
            z_copy(d, h).wait_recv()
            total = total + rzz[at(d, h)].astype(f32)
        scale = lax.rsqrt(jnp.mean(total * total, axis=-1, keepdims=True) + epsilon)
        out[h * piece : (h + 1) * piece, :] = (total * scale * post[...]).astype(out.dtype)
    for copy in started:
        copy.wait_send()


def body(tokens, routing, gate_weights, pre_gain, w_gate, w_up, w_down, post_gain):
    n = lax.axis_size("ep")
    rows, width = tokens.shape
    ff = w_gate.shape[2]
    zs = n // 4
    parts = 2 if rows % 32 == 0 and zs <= 4 else 1
    piece, count = rows // parts, zs * parts
    extra = -(-2 * n // 128) * 128
    bf16, dma = jnp.bfloat16, pltpu.SemaphoreType.DMA
    vmem = pl.BlockSpec(memory_space=pltpu.VMEM)
    hbm = pl.BlockSpec(memory_space=pl.ANY)
    return pl.pallas_call(
        functools.partial(kernel, n, parts),
        out_shape=jax.ShapeDtypeStruct((rows, width), bf16),
        in_specs=[vmem, vmem, vmem, vmem, hbm, hbm, hbm, vmem],
        out_specs=vmem,
        scratch_shapes=[
            pltpu.VMEM((parts, n, piece, width + extra), bf16),
            pltpu.VMEM((count, 4, piece, width), bf16),
            pltpu.VMEM((count, 2, piece, width), bf16),
            pltpu.VMEM((count, piece, width), bf16),
            pltpu.VMEM((count, piece, width), bf16),
            pltpu.VMEM((count, piece, width), bf16),
            pltpu.VMEM((count, piece, width), bf16),
            pltpu.VMEM((parts, piece, width), jnp.float32),
            pltpu.VMEM((width, ff), bf16),
            pltpu.VMEM((width, ff), bf16),
            pltpu.VMEM((ff, width), bf16),
            dma((4 * count,)), dma((4 * count,)),
            dma((2 * count,)), dma((2 * count,)),
            dma((count,)), dma((count,)), dma((count,)), dma((count,)),
            dma((3,)),
        ],
        compiler_params=pltpu.CompilerParams(
            collective_id=0, has_side_effects=True, vmem_limit_bytes=60 * 1024 * 1024
        ),
    )(
        tokens, routing.T, gate_weights.T, pre_gain.reshape(1, width),
        w_gate, w_up, w_down, post_gain.reshape(1, width),
    )


def solution(mesh):
    rows = P(("grp", "ep"), None)
    expert = P("ep", None, None)
    in_specs = (rows, rows, rows, P(), expert, expert, expert, P())
    return jax.shard_map(body, mesh=mesh, in_specs=in_specs, out_specs=rows, check_vma=False)
```

time: 47.7 us -> 46.8 us (0.981)
  the two profiles are of different devices: /device:TPU:11 before, /device:TPU:0 now
where the time goes in v2:
time: 46.8 us; the launch traced here: 46.7 us
  Pallas kernels  45.1 us (96%)
  local copies, waits for them, and re-layouts  1.57 us (3%)
    pallas_call x1, Pallas kernels, body(): pl.pallas_call(functools.partial(kernel, n, parts), out_shape=jax.ShapeDt...  45.1 us
    unnamed x1, local copies, waits for them, and re-layouts  1.57 us

profile of v2, /device:TPU:0, one launch (start us, length us, event | category | flops | bytes accessed | tf_op | source)
XLA Modules:
  0.0 46.7 jit_solution(15624035765481468613)
XLA Ops:
  0.0 45.1 %shard_map.82 = bf16[32,2048]{1,0:T(8,128)(2,1)} custom-call(bf16[32,2048]{1,0:T(8,128)(2,1)} %tok.1, s32[4,32]{1,0:T(4,128)} %bitcast.6, f32[4,32]{1,0:T(4,128)} %bitcast.7, f32[1,2048]{1,0:T(1,128)} %bitcast.4, bf16[1,2048,512]{2,1,0:T(8,128)(2,1)} %wg_hbm.1, bf16[1,2048,512]{2,1,0:T(8,128)(2,1)} %wu_hbm.1, bf16[1,512,2048]{2,1,0:T(8,128)(2,1)} %wd_hbm.1, ...), custom_call_target="tpu_custom_call" | custom-call | tf_op jit(solution)/shard_map/pallas_call | solution.py:200
  45.1 1.6 %copy.10 = bf16[32,2048]{1,0:T(8,128)(2,1)} copy(bf16[32,2048]{1,0:T(8,128)(2,1)} %shard_map.82) | data formatting | bytes 262144

commit v3 on v2

--- a/solution.py
+++ b/solution.py
@@ -152,7 +152,7 @@
             zsend[i] = total.astype(bf16)
             go(z_copy(d, h))
 
-    order = ([0, 1] + list(range(2, zs))[::-1])[:zs]
+    order = list(range(zs))
     steps = [(d, h) for d in order for h in range(parts)]
 
     for h in range(parts):
@@ -191,7 +191,7 @@
     rows, width = tokens.shape
     ff = w_gate.shape[2]
     zs = n // 4
-    parts = 2 if rows % 32 == 0 and zs <= 4 else 1
+    parts = 1
     piece, count = rows // parts, zs * parts
     extra = -(-2 * n // 128) * 128
     bf16, dma = jnp.bfloat16, pltpu.SemaphoreType.DMA

time: 46.8 us -> 44.8 us (0.957)
  the two profiles are of different devices: /device:TPU:0 before, /device:TPU:11 now
where the time goes in v3:
time: 44.8 us; the launch traced here: 44.1 us
  Pallas kernels  42.5 us (95%)
  local copies, waits for them, and re-layouts  1.57 us (4%)
    pallas_call x1, Pallas kernels, body(): pl.pallas_call(functools.partial(kernel, n, parts), out_shape=jax.ShapeDt...  42.5 us
    unnamed x1, local copies, waits for them, and re-layouts  1.57 us

profile of v3, /device:TPU:11, one launch (start us, length us, event | category | flops | bytes accessed | tf_op | source)
XLA Modules:
  0.0 44.1 jit_solution(15531608159918707406)
XLA Ops:
  0.0 42.5 %shard_map.82 = bf16[32,2048]{1,0:T(8,128)(2,1)} custom-call(bf16[32,2048]{1,0:T(8,128)(2,1)} %tok.1, s32[4,32]{1,0:T(4,128)} %bitcast.6, f32[4,32]{1,0:T(4,128)} %bitcast.7, f32[1,2048]{1,0:T(1,128)} %bitcast.4, bf16[1,2048,512]{2,1,0:T(8,128)(2,1)} %wg_hbm.1, bf16[1,2048,512]{2,1,0:T(8,128)(2,1)} %wu_hbm.1, bf16[1,512,2048]{2,1,0:T(8,128)(2,1)} %wd_hbm.1, ...), custom_call_target="tpu_custom_call" | custom-call | tf_op jit(solution)/shard_map/pallas_call | solution.py:200
  42.5 1.6 %copy.10 = bf16[32,2048]{1,0:T(8,128)(2,1)} copy(bf16[32,2048]{1,0:T(8,128)(2,1)} %shard_map.82) | data formatting | bytes 262144
